TPU v7x, 32 devices: a whole 2x2x4 slice. The times are simulated.
32 devices in a mesh: sp: 8 (over z, y), tp: 4 (over x, core).
Axes of the slice: x: 2, y: 2, z: 4, core: 2. Of those that a mesh axis runs over, the one named last changes fastest.
Arguments:
- proj_value: bfloat16 [4096, 2016], P('sp', 'tp'), may hold values from -6 to 6
- proj_gate: bfloat16 [4096, 2016], P('sp', 'tp'), may hold values from -8 to 8
- conv_saved: bfloat16 [4096, 2016], P('sp', 'tp'), may hold values from -12 to 12
- conv_taps: bfloat16 [31, 2016], P(None, 'tp'), may hold values from -1 to 1
- norm_gain: bfloat16 [2016], P('tp'), may hold values from 0.099609375 to 1.8984375
- out_weight: bfloat16 [2016, 2016], P('tp'), may hold values from -0.125 to 0.125
- cotangent: bfloat16 [4096, 2016], P('sp'), may hold values from -6 to 6
Outputs:
- grad_value: bfloat16 [4096, 2016], P('sp', 'tp')
- grad_gate: bfloat16 [4096, 2016], P('sp', 'tp')
- grad_out_weight: float32 [2016, 2016], P('tp', 'sp')
- grad_taps: float32 [31, 2016], P(None, 'tp')
All inputs are finite; a program needn't handle non-finite values.
Results may differ from a plain program's by a relative error of at most 0.003.
Values sent between devices are 32-bit elements; how exact they have to be, the bound alone decides.
A program may use at most 64 MiB of HBM per device.

v0:
```python
import math

import jax
import jax.numpy as jnp
from jax import lax
from jax.sharding import PartitionSpec as P

norm_eps = 1e-05


def passed_along(block, axis, distance):
    devices = range(lax.axis_size(axis))
    route = [(i - distance, i) for i in devices if i - distance in devices]
    return lax.ppermute(block, axis, route)


def local(proj_value, proj_gate, conv_saved, conv_taps, norm_gain, out_weight, cotangent):
    model_width = cotangent.shape[1]
    tok_rows = cotangent.shape[0]
    tap_count = conv_taps.shape[0]
    overhang = tap_count - 1
    grad_scale = 1.0 / math.sqrt(tok_rows * lax.axis_size("sp"))
    conv_f = conv_saved.astype(jnp.float32)
    totals = lax.psum((jnp.sum(conv_f, axis=1), jnp.sum(conv_f * conv_f, axis=1)), "tp")
    row_mean = totals[0] / model_width
    row_var = totals[1] / model_width - row_mean * row_mean
    inv_std = lax.rsqrt(row_var + norm_eps)
    centered = (conv_f - row_mean[:, None]) * inv_std[:, None]
    gain_f = norm_gain.astype(jnp.float32)
    normed = centered * gain_f
    gate_norm = jax.nn.sigmoid(normed)
    activated = (normed * gate_norm).astype(jnp.bfloat16)
    contract_rows = (((0,), (0,)), ((), ()))
    whole_term = lax.dot_general(
        cotangent, activated, contract_rows, preferred_element_type=jnp.float32
    )
    shard_grad = lax.psum_scatter(whole_term, "sp", scatter_dimension=0, tiled=True)
    grad_out_weight = shard_grad.T * grad_scale
    d_act = lax.dot_general(
        cotangent, out_weight, (((1,), (1,)), ((), ())), preferred_element_type=jnp.float32
    )
    d_hat = d_act * gate_norm * (1.0 + normed * (1.0 - gate_norm)) * gain_f
    moments = lax.psum((jnp.sum(d_hat, axis=1), jnp.sum(d_hat * centered, axis=1)), "tp")
    first = moments[0] / model_width
    second = moments[1] / model_width
    d_conv = inv_std[:, None] * (d_hat - first[:, None] - centered * second[:, None])
    ahead = passed_along(d_conv[:overhang], "sp", -1)
    extended = jnp.concatenate([d_conv, ahead], axis=0)
    gate_proj = jax.nn.sigmoid(proj_gate.astype(jnp.float32))
    gated = proj_value.astype(jnp.float32) * gate_proj
    taps_f = conv_taps.astype(jnp.float32)
    d_glu = jnp.zeros_like(d_conv)
    tap_rows = []
    for offset in range(tap_count):
        shifted = extended[overhang - offset : overhang - offset + tok_rows]
        d_glu = d_glu + taps_f[offset] * shifted
        tap_rows.append(jnp.sum(gated * shifted, axis=0))
    grad_taps = lax.psum(jnp.stack(tap_rows), "sp") * grad_scale
    grad_value = (d_glu * gate_proj).astype(jnp.bfloat16)
    grad_gate = (d_glu * gated * (1.0 - gate_proj)).astype(jnp.bfloat16)
    return (grad_value, grad_gate, grad_out_weight, grad_taps)


def solution(mesh):
    in_specs = (
        P("sp", "tp"),
        P("sp", "tp"),
        P("sp", "tp"),
        P(None, "tp"),
        P("tp"),
        P("tp", None),
        P("sp", None),
    )
    out_specs = (P("sp", "tp"), P("sp", "tp"), P("tp", "sp"), P(None, "tp"))
    return jax.shard_map(local, mesh=mesh, in_specs=in_specs, out_specs=out_specs, check_vma=False)
```

profile of v0, /device:TPU:12, one launch (start us, length us, event | category | flops | bytes accessed | tf_op | source)
XLA Modules:
  0.0 197.9 jit_solution(5492101719931383703)
XLA Ops:
  7.2 0.0 copy-start
  7.2 0.0 all-reduce.5.cloned.1.call-start
  7.2 1.3 fusion.2
  8.6 0.7 convert_element_type.26
  9.3 6.9 %all-reduce.2 = (f32[512]{0:T(512)S(1)}, f32[512]{0:T(512)S(1)}) all-reduce(f32[512]{0:T(512)S(1)} %get-tuple-element.38, f32[512]{0:T(512)S(1)} %get-tuple-element.37), channel_id=1, replica_groups=mesh['sp'=8,'tp'=4] {'tp'}, use_global_device_ids=true, to_apply=%region_3.0 | all-reduce | flops 1024 | bytes 8192 | tf_op jit(solution)/shard_map/psum | solution.py:24
  16.1 0.0 copy-done
  16.1 4.3 %fusion.54 = (f32[512]{0:T(512)S(1)}, f32[512]{0:T(512)S(1)}, f32[512,504]{0,1:T(8,128)}) fusion(f32[512]{0:T(512)S(1)} %get-tuple-element.77, f32[512]{0:T(512)S(1)} %get-tuple-element.78, bf16[512,504]{0,1:T(8,128)(2,1)} %param.9, f32[504]{0:T(512)S(1)} %convert_element_type.26, bf16[512,2016]{0,1:T(8,128)(2,1)S(1)} %copy-done, bf16[504,2016]{1,0:T(8,128)(2,1)} %param.12), kind=kOutput, calls=%fused_computation.159 | convolution fusion | flops 1044577280 | bytes 5655008 | tf_op jit(solution)/shard_map/dot_general | solution.py:39
  20.4 5.8 %all-reduce.1 = (f32[512]{0:T(512)S(1)}, f32[512]{0:T(512)S(1)}) all-reduce(f32[512]{0:T(512)S(1)} %get-tuple-element.36, f32[512]{0:T(512)S(1)} %get-tuple-element.35), channel_id=1, replica_groups=mesh['sp'=8,'tp'=4] {'tp'}, use_global_device_ids=true, to_apply=%region_7.0 | all-reduce | flops 1024 | bytes 8192 | tf_op jit(solution)/shard_map/psum | solution.py:43
  26.3 0.0 copy-start.3
  26.3 1.7 fusion.17
  27.9 0.7 slice.249
  28.7 2.6 %collective-permute-start = (f32[30,504]{0,1:T(8,128)}, f32[30,504]{0,1:T(8,128)S(1)}, u32[]{:S(2)}, u32[]{:S(2)}) collective-permute-start(f32[30,504]{0,1:T(8,128)} %slice.249), channel_id=1, source_target_pairs={{4,0},{8,4},{12,8},{16,12},{20,16},{24,20},{28,24},{5,1},{9,5},{13... | collective-permute-start | bytes 181448 | tf_op jit(solution)/shard_map/ppermute | solution.py:14
  31.3 0.0 copy-done.3
  31.3 3.4 %convolution_bitcast_fusion = f32[2016,504]{0,1:T(8,128)} fusion(bf16[512,2016]{0,1:T(8,128)(2,1)S(1)} %copy-done, bf16[512,504]{0,1:T(8,128)(2,1)S(1)} %copy-done.3, f32[504]{0:T(512)S(1)} %convert_element_type.26, f32[512]{0:T(512)S(1)} %get-tuple-element.78, f32[512]{0:T(512)S(1)} %get-tuple-element.77), kind=kOutput, calls=%fused_computation.29 | convolution fusion | flops 1042771968 | bytes 6650848 | tf_op jit(solution)/shard_map/dot_general | solution.py:34
  34.7 0.0 copy-start.4
  34.7 0.0 copy-start.5
  34.7 0.0 all-reduce.5.cloned.1.call-update
  34.7 0.7 copy-done.4
  35.5 0.0 copy-done.5
  35.5 0.6 dynamic-slice
  36.8 2.7 %collective-permute-done = f32[30,504]{0,1:T(8,128)S(1)} collective-permute-done((f32[30,504]{0,1:T(8,128)}, f32[30,504]{0,1:T(8,128)S(1)}, u32[]{:S(2)}, u32[]{:S(2)}) %collective-permute-start) | collective-permute-done | bytes 60512 | tf_op jit(solution)/shard_map/ppermute | solution.py:14
  39.4 0.0 copy-start.1
  39.4 0.0 copy-start.2
  39.4 17.6 %multiply_convert_fusion = (bf16[512,504]{0,1:T(8,128)(2,1)}, f32[512,504]{0,1:T(8,128)S(1)}) fusion(bf16[512,504]{0,1:T(8,128)(2,1)} %param.8, bf16[512,504]{0,1:T(8,128)(2,1)} %param.7, f32[512,504]{0,1:T(8,128)S(1)} %fusion.17, f32[504]{0:T(512)S(1)} %bitcast.109, f32[30,504]{0,1:T(8,128)S(1)} %collective-permute-done, f32[504]{0:T(512)S(1)} %bitcast.108, ...), kind=kLoop, calls=%fused_computation.142 | loop fusion | flops 26062848 | bytes 3735648 | tf_op jit(solution)/shard_map/convert_element_type | solution.py:60
  57.1 0.0 copy-done.1
  57.1 0.0 copy-done.2
  57.1 4.1 %multiply_reduce_fusion.4 = (f32[504]{0:T(512)S(1)}, f32[504]{0:T(512)S(1)}, f32[504]{0:T(512)S(1)}, f32[504]{0:T(512)S(1)}, f32[504]{0:T(512)S(1)}, /*index=5*/...) fusion(f32[30,504]{0,1:T(8,128)S(1)} %collective-permute-done, f32[512,504]{0,1:T(8,128)S(1)} %fusion.17, ...), kind=kLoop, calls=%fused_computation.115 | loop fusion | flops 7221816 | bytes 3687264 | tf_op jit(solution)/shard_map/reduce_sum | solution.py:57
  61.2 4.3 %multiply_reduce_fusion.1 = (f32[504]{0:T(512)S(1)}, f32[504]{0:T(512)S(1)}, f32[504]{0:T(512)S(1)}, f32[504]{0:T(512)S(1)}, f32[504]{0:T(512)S(1)}, /*index=5*/f32[504]{0:T(512)S(1)}, f32[504]{0:T(512)S(1)}, f32[504]{0:T(512)S(1)}) fusion(f32[30,504]{0,1:T(8,128)S(1)} %collective-permute-done, f32[512,504]{0,1:T(8,128)S(1)} %fusion.17, ...), kind=kLoop, calls=%fused_computation.112 | loop fusion | flops 7737408 | bytes 2140992 | tf_op jit(solution)/shard_map/reduce_sum | solution.py:57
  65.5 4.4 %multiply_reduce_fusion.2 = (f32[504]{0:T(512)S(1)}, f32[504]{0:T(512)S(1)}, f32[504]{0:T(512)S(1)}, f32[504]{0:T(512)S(1)}, f32[504]{0:T(512)S(1)}, /*index=5*/f32[504]{0:T(512)S(1)}, f32[504]{0:T(512)S(1)}, f32[504]{0:T(512)S(1)}) fusion(f32[30,504]{0,1:T(8,128)S(1)} %collective-permute-done, f32[512,504]{0,1:T(8,128)S(1)} %fusion.17, ...), kind=kLoop, calls=%fused_computation.113 | loop fusion | flops 7737408 | bytes 2140992 | tf_op jit(solution)/shard_map/reduce_sum | solution.py:57
  69.9 4.4 %multiply_reduce_fusion.3 = (f32[504]{0:T(512)S(1)}, f32[504]{0:T(512)S(1)}, f32[504]{0:T(512)S(1)}, f32[504]{0:T(512)S(1)}, f32[504]{0:T(512)S(1)}, /*index=5*/f32[504]{0:T(512)S(1)}, f32[504]{0:T(512)S(1)}, f32[504]{0:T(512)S(1)}) fusion(f32[30,504]{0,1:T(8,128)S(1)} %collective-permute-done, f32[512,504]{0,1:T(8,128)S(1)} %fusion.17, ...), kind=kLoop, calls=%fused_computation.114 | loop fusion | flops 7737408 | bytes 2140992 | tf_op jit(solution)/shard_map/reduce_sum | solution.py:57
  74.2 0.1 stack.127
  74.4 30.1 %psum.39 = f32[31,504]{1,0:T(8,128)S(1)} all-reduce(f32[31,504]{1,0:T(8,128)S(1)} %stack.127), channel_id=1, replica_groups=mesh['sp'=8,'tp'=4] {'sp'}, use_global_device_ids=true, to_apply=%region_40.0 | all-reduce | flops 15624 | bytes 124992 | tf_op jit(solution)/shard_map/psum | solution.py:58
  104.5 0.6 broadcast_multiply_fusion
  105.1 83.8 %all-reduce.5.cloned.1.call-done = f32[2016,504]{0,1:T(8,128)} async-done(((f32[2016,504]{0,1:T(8,128)}), f32[2016,504]{0,1:T(8,128)}) %all-reduce.5.cloned.1.call-update) | async-done | bytes 4064272
  188.9 2.1 %fusion.48 = f32[504,252]{1,0:T(8,128)} fusion(f32[2016,504]{0,1:T(8,128)} %all-reduce.5.cloned.1.call-done, u32[]{:T(128)S(6)} %multiply.5), kind=kLoop, calls=%fused_computation.148 | loop fusion | flops 127008 | bytes 1016068 | tf_op jit(solution)/shard_map/mul | solution.py:38
  (4 shorter events, 0.1 us)
Async XLA Ops:
  7.2 9.0 %copy-start = (bf16[512,2016]{0,1:T(8,128)(2,1)S(1)}, bf16[512,2016]{0,1:T(8,128)(2,1)}, u32[]{:S(2)}) copy-start(bf16[512,2016]{0,1:T(8,128)(2,1)} %param.13) | copy-start | bytes 6193156
  7.2 181.7 %all-reduce.5.cloned.1.call-start = ((), (), s32[]{:S(2)}) async-start(), calls=%async_computation | async-start | bytes 8257536
  26.3 5.0 %copy-start.3 = (bf16[512,504]{0,1:T(8,128)(2,1)S(1)}, bf16[512,504]{0,1:T(8,128)(2,1)}, u32[]{:S(2)}) copy-start(bf16[512,504]{0,1:T(8,128)(2,1)} %param.9) | copy-start | bytes 1548292
  28.7 10.8 %collective-permute-start = (f32[30,504]{0,1:T(8,128)}, f32[30,504]{0,1:T(8,128)S(1)}, u32[]{:S(2)}, u32[]{:S(2)}) collective-permute-start(f32[30,504]{0,1:T(8,128)} %slice.249), channel_id=1, source_target_pairs={{4,0},{8,4},{12,8},{16,12},{20,16},{24,20},{28,24},{5,1},{9,5},{13... | collective-permute-start | bytes 181448 | tf_op jit(solution)/shard_map/ppermute | solution.py:14
  34.7 0.8 copy-start.4
  34.7 0.8 copy-start.5
  39.4 17.6 %copy-start.1 = (bf16[512,504]{0,1:T(8,128)(2,1)S(1)}, bf16[512,504]{0,1:T(8,128)(2,1)}, u32[]{:S(2)}) copy-start(bf16[512,504]{0,1:T(8,128)(2,1)} %param.8) | copy-start | bytes 1548292
  39.4 17.6 %copy-start.2 = (bf16[512,504]{0,1:T(8,128)(2,1)S(1)}, bf16[512,504]{0,1:T(8,128)(2,1)}, u32[]{:S(2)}) copy-start(bf16[512,504]{0,1:T(8,128)(2,1)} %param.7) | copy-start | bytes 1548292
Sparse Core Ops, SparseCore 0:
  34.9 154.0 all-reduce.4
where the time goes:
time: 201 us; the launch traced here: 198 us
  waiting for transfers between devices  86.4 us (43%)
  blocking collectives  42.8 us (21%)
  other arithmetic  41.3 us (21%)
  between operations  14.8 us (7%)
  matrix products  7.72 us (4%)
  starting transfers between devices  2.62 us (1%)
  local copies, waits for them, and re-layouts  2.27 us (1%)
    unnamed x2, waiting for transfers between devices  83.8 us
    psum x1, blocking collectives, local(): grad_taps = lax.psum(jnp.stack(tap_rows), 'sp') * grad_scale  30.1 us
    convert_element_type x1, other arithmetic, local(): grad_gate = (d_glu * gated * (1.0 - gate_proj)).astype(jnp.bfloat16)  17.6 us
    reduce_sum x4, other arithmetic, local(): tap_rows.append(jnp.sum(gated * shifted, axis=0))  17.2 us
    psum x1, blocking collectives, local(): lax.psum((jnp.sum(conv_f, axis=1), jnp.sum(conv_f * conv_f, axis=1)), 'tp')  6.86 us
    psum x1, blocking collectives, local(): lax.psum((jnp.sum(d_hat, axis=1), jnp.sum(d_hat * centered, axis=1)), 'tp')  5.85 us
    dot_general x1, matrix products, local(): lax.dot_general(cotangent, out_weight, (((1,), (1,)), ((), ())), preferre...  4.27 us
  transfers between devices with their start and end apart: 2, of which 2 were waited for; matrix products, arithmetic and copies ran while one was open for 20% of the time, Pallas kernels for 0%

commit v1 on v0

--- a/solution.py
+++ b/solution.py
@@ -1,11 +1,388 @@
+import functools
 import math
 
 import jax
 import jax.numpy as jnp
 from jax import lax
+from jax.experimental import pallas as pl
+from jax.experimental.pallas import tpu as pltpu
 from jax.sharding import PartitionSpec as P
 
 norm_eps = 1e-05
+MESH = pl.DeviceIdType.MESH
+f32 = jnp.float32
+
+
+def line_order(length):
+    rows = []
+    for place in range(length):
+        side = 1 if 2 * place >= length else -1
+        rows.append(sorted(range(length), key=lambda d: (-abs(d - place), -side * (d - place))))
+    return rows
+
+
+def lookup(table, place):
+    value = table[0]
+    for i in range(1, len(table)):
+        value = jnp.where(place == i, table[i], value)
+    return value
+
+
+def kernel(
+    n_sp, n_tp, fold, pv, pg, conv, taps, gain, weight, cot,
+    out_v, out_g, out_w, out_t,
+    act_t, d_act, ext, shifted, cols, cols2, term, got_y, got_r, got_l,
+    stat, stat_in, mom, mom_in, grad_acc, g_own, g_mid, g_in, g_yin, taps_b,
+    stat_ss, stat_rs, mom_ss, mom_rs, y_ss, y_rs, r_ss, r_rs, l_ss, l_rs,
+    halo_ss, halo_rs, gz_ss, gz_rs, gy_ss, gy_rs,
+):
+    s = lax.axis_index("sp")
+    t = lax.axis_index("tp")
+    n_z = n_sp // fold
+    z = s // fold
+    y = s % fold
+    other_y = 1 - y
+    rows, width = cot.shape
+    ch = conv.shape[1]
+    part = out_w.shape[1]
+    n_taps = taps.shape[0]
+    scale = 1.0 / math.sqrt(rows * n_sp)
+    blk = 128
+    n_blk = rows // blk
+
+    barrier = pltpu.get_barrier_semaphore()
+    for i in range(1, n_sp):
+        pl.semaphore_signal(barrier, inc=1, device_id=(lax.rem(s + i, n_sp), t), device_id_type=MESH)
+    for i in range(1, n_tp):
+        pl.semaphore_signal(barrier, inc=1, device_id=(s, lax.rem(t + i, n_tp)), device_id_type=MESH)
+
+    def pack(a, b):
+        lane = lax.broadcasted_iota(jnp.int32, (blk, blk), 1)
+        return jnp.where(lane == 0, a, b).T[:8]
+
+    def unpack(x):
+        return jnp.concatenate([x] * (blk // 8), axis=0).T
+
+    @pl.loop(0, n_blk)
+    def _(i):
+        at = pl.ds(pl.multiple_of(i * blk, blk), blk)
+        c = conv[at, :].astype(f32)
+        stat[:, at] = pack(jnp.sum(c, axis=1, keepdims=True), jnp.sum(c * c, axis=1, keepdims=True))
+
+    pl.semaphore_wait(barrier, n_sp - 1 + n_tp - 1)
+
+    def tp_copies(src, dst, ss, rs):
+        return [
+            pltpu.make_async_remote_copy(
+                src_ref=src, dst_ref=dst.at[i - 1], send_sem=ss.at[i - 1], recv_sem=rs.at[i - 1],
+                device_id=(s, lax.rem(t + i, n_tp)), device_id_type=MESH,
+            )
+            for i in range(1, n_tp)
+        ]
+
+    stat_copies = tp_copies(stat, stat_in, stat_ss, stat_rs)
+    for c in stat_copies:
+        c.start()
+
+    @pl.loop(0, n_blk)
+    def _(i):
+        at = pl.ds(pl.multiple_of(i * blk, blk), blk)
+        d_act[at, :] = lax.dot_general(
+            cot[at, :], weight[...], (((1,), (1,)), ((), ())), preferred_element_type=f32
+        )
+
+    for c in stat_copies:
+        c.wait()
+    total = stat[...]
+    for i in range(n_tp - 1):
+        total = total + stat_in[i]
+    mean = total[0:1] / width
+    inv = lax.rsqrt(total[1:2] / width - mean * mean + norm_eps)
+    row8 = lax.broadcasted_iota(jnp.int32, (8, rows), 0)
+    both = jnp.where(row8 == 0, mean, inv)
+    for i in range(n_blk):
+        cols[i * blk:(i + 1) * blk, :] = unpack(both[:, i * blk:(i + 1) * blk])
+
+    gain_f = gain[...].astype(f32)
+
+    @pl.loop(0, n_blk)
+    def _(i):
+        at = pl.ds(pl.multiple_of(i * blk, blk), blk)
+        c = conv[at, :].astype(f32)
+        normed = (c - cols[at, 0:1]) * cols[at, 1:2] * gain_f
+        a = normed * jax.nn.sigmoid(normed)
+        act_t[:, at] = a.T.astype(jnp.bfloat16)
+
+    for j in range(n_sp):
+        term[j] = jnp.dot(act_t[...], cot[:, j * part:(j + 1) * part], preferred_element_type=f32)
+
+    orders = line_order(n_z)
+    dest = [lookup([orders[i][k] for i in range(n_z)], z) for k in range(n_z)]
+
+    def y_copy(k):
+        return pltpu.make_async_remote_copy(
+            src_ref=term.at[dest[k] * fold + other_y], dst_ref=got_y.at[dest[k]],
+            send_sem=y_ss.at[dest[k]], recv_sem=y_rs.at[dest[k]],
+            device_id=(z * fold + other_y, t), device_id_type=MESH,
+        )
+
+    y_copies = [y_copy(k) for k in range(n_z)]
+
+    def line_copy(d, up):
+        buf, ss, rs = (got_r, r_ss, r_rs) if up else (got_l, l_ss, l_rs)
+        to = z + 1 if up else z - 1
+        to = jnp.clip(to, 0, n_z - 1)
+        return pltpu.make_async_remote_copy(
+            src_ref=term.at[d * fold + y], dst_ref=buf.at[d], send_sem=ss.at[d], recv_sem=rs.at[d],
+            device_id=(to * fold + y, t), device_id_type=MESH,
+        )
+
+    def add_into(d, buf):
+        own = d * fold + y
+        step = 56 if ch % 56 == 0 else 8
+
+        @pl.loop(0, ch // step)
+        def _(i):
+            at = pl.ds(pl.multiple_of(i * step, 8), step)
+            term[own, at, :] = term[own, at, :] + buf[d, at, :]
+
+    def hop(k):
+        d = dest[k]
+        y_copies[k].wait_recv()
+        add_into(d, got_y)
+
+        @pl.when(d > z)
+        def _():
+            @pl.when(z > 0)
+            def _():
+                line_copy(d, True).wait_recv()
+                add_into(d, got_r)
+
+            line_copy(d, True).start()
+
+        @pl.when(d < z)
+        def _():
+            @pl.when(z < n_z - 1)
+            def _():
+                line_copy(d, False).wait_recv()
+                add_into(d, got_l)
+
+            line_copy(d, False).start()
+
+    y_copies[0].start()
+    y_copies[1].start()
+
+    @pl.loop(0, n_blk)
+    def _(i):
+        at = pl.ds(pl.multiple_of(i * blk, blk), blk)
+        c = conv[at, :].astype(f32)
+        centered = (c - cols[at, 0:1]) * cols[at, 1:2]
+        normed = centered * gain_f
+        gate = jax.nn.sigmoid(normed)
+        d_hat = d_act[at, :] * gate * (1.0 + normed * (1.0 - gate)) * gain_f
+        d_act[at, :] = d_hat
+        mom[:, at] = pack(
+            jnp.sum(d_hat, axis=1, keepdims=True), jnp.sum(d_hat * centered, axis=1, keepdims=True)
+        )
+
+    mom_copies = tp_copies(mom, mom_in, mom_ss, mom_rs)
+    for c in mom_copies:
+        c.start()
+    for k in range(n_taps):
+        taps_b[k] = jnp.broadcast_to(taps[k:k + 1, :].astype(f32), (8, ch))
+    grad_acc[...] = jnp.zeros_like(grad_acc)
+    for c in mom_copies:
+        c.wait()
+    total = mom[...]
+    for i in range(n_tp - 1):
+        total = total + mom_in[i]
+    total = total / width
+    for i in range(n_blk):
+        cols2[i * blk:(i + 1) * blk, :] = unpack(total[:, i * blk:(i + 1) * blk])
+
+    @pl.loop(0, n_blk)
+    def _(i):
+        at = pl.ds(pl.multiple_of(i * blk, blk), blk)
+        c = conv[at, :].astype(f32)
+        inv_std = cols[at, 1:2]
+        centered = (c - cols[at, 0:1]) * inv_std
+        ext[at, :] = inv_std * (d_act[at, :] - cols2[at, 0:1] - centered * cols2[at, 1:2])
+
+    reach = 32
+    back = jnp.maximum(s - 1, 0)
+    halo = pltpu.make_async_remote_copy(
+        src_ref=ext.at[pl.ds(0, reach), :], dst_ref=ext.at[pl.ds(rows, reach), :],
+        send_sem=halo_ss, recv_sem=halo_rs, device_id=(back, t), device_id_type=MESH,
+    )
+
+    @pl.when(s > 0)
+    def _():
+        halo.start()
+
+    for k in range(2, n_z):
+        y_copies[k].start()
+
+    def shift_block(i):
+        start = pl.multiple_of(i * reach, reach)
+        win = ext[pl.ds(start, reach + 8), :]
+        for o in range(8):
+            shifted[o, pl.ds(start, reach), :] = win[o:o + reach]
+
+    lanes = [(lo, min(128, ch - lo)) for lo in range(0, ch, 128)]
+
+    def conv_blocks(first, last):
+        for lo, wide in lanes:
+            ln = slice(lo, lo + wide)
+
+            def body(i, accs):
+                start = pl.multiple_of(i * reach, reach)
+                at = pl.ds(start, reach)
+                gate = jax.nn.sigmoid(pg[at, ln].astype(f32))
+                gated = pv[at, ln].astype(f32) * gate
+                d_glu = jnp.zeros((reach, wide), f32)
+                out = []
+                for o in range(n_taps):
+                    x = shifted[o % 8, pl.ds(pl.multiple_of(start + 8 * (o // 8), 8), reach), ln]
+                    tap = taps_b[n_taps - 1 - o, :, ln]
+                    d_glu = d_glu + jnp.concatenate([tap] * (reach // 8), axis=0) * x
+                    prod = gated * x
+                    acc = accs[o]
+                    for q in range(reach // 8):
+                        acc = acc + prod[8 * q:8 * q + 8]
+                    out.append(acc)
+                out_v[at, ln] = (d_glu * gate).astype(jnp.bfloat16)
+                out_g[at, ln] = (d_glu * gated * (1.0 - gate)).astype(jnp.bfloat16)
+                return tuple(out)
+
+            accs = tuple(grad_acc[n_taps - 1 - o, :, ln] for o in range(n_taps))
+            accs = lax.fori_loop(first, last, body, accs)
+            for o in range(n_taps):
+                grad_acc[n_taps - 1 - o, :, ln] = accs[o]
+
+    n_row = rows // reach
+
+    @pl.loop(0, n_row - 1)
+    def _(i):
+        shift_block(i)
+
+    hop(0)
+    half = (n_row - 2) // 2
+    conv_blocks(0, half)
+    hop(1)
+    conv_blocks(half, n_row - 2)
+
+    @pl.when(s < n_sp - 1)
+    def _():
+        halo.wait_recv()
+
+    @pl.when(s == n_sp - 1)
+    def _():
+        ext[pl.ds(rows, reach), :] = jnp.zeros((reach, ch), f32)
+
+    shift_block(n_row - 1)
+    win = ext[pl.ds(rows, reach), :]
+    for o in range(8):
+        shifted[o, pl.ds(rows, reach - 8), :] = win[o:o + reach - 8]
+    conv_blocks(n_row - 2, n_row)
+
+    for k in range(n_taps):
+        g_own[k:k + 1, :] = jnp.sum(grad_acc[k], axis=0, keepdims=True)
+    for k in range(n_taps, g_own.shape[0]):
+        g_own[k:k + 1, :] = jnp.zeros((1, ch), f32)
+    gz_copies = [
+        pltpu.make_async_remote_copy(
+            src_ref=g_own, dst_ref=g_in.at[i - 1], send_sem=gz_ss.at[i - 1], recv_sem=gz_rs.at[i - 1],
+            device_id=(lax.rem(z + i, n_z) * fold + y, t), device_id_type=MESH,
+        )
+        for i in range(1, n_z)
+    ]
+    for c in gz_copies:
+        c.start()
+    for k in range(2, n_z - 1):
+        hop(k)
+    for c in gz_copies:
+        c.wait()
+    total = g_own[...]
+    for i in range(n_z - 1):
+        total = total + g_in[i]
+    g_mid[...] = total
+    gy = pltpu.make_async_remote_copy(
+        src_ref=g_mid, dst_ref=g_yin, send_sem=gy_ss, recv_sem=gy_rs,
+        device_id=(z * fold + other_y, t), device_id_type=MESH,
+    )
+    gy.start()
+    y_copies[n_z - 1].wait_recv()
+    add_into(z, got_y)
+
+    @pl.when(z > 0)
+    def _():
+        line_copy(z, True).wait_recv()
+        add_into(z, got_r)
+
+    @pl.when(z < n_z - 1)
+    def _():
+        line_copy(z, False).wait_recv()
+        add_into(z, got_l)
+
+    out_w[...] = term[z * fold + y] * scale
+    gy.wait()
+    out_t[...] = ((g_mid[...] + g_yin[...]) * scale)[:n_taps]
+    for k in range(n_z):
+        y_copies[k].wait_send()
+
+    @pl.when(s > 0)
+    def _():
+        halo.wait_send()
+
+    for k in range(n_z - 1):
+        d = dest[k]
+
+        @pl.when(d > z)
+        def _():
+            line_copy(d, True).wait_send()
+
+        @pl.when(d < z)
+        def _():
+            line_copy(d, False).wait_send()
+
+
+def fused(n_sp, n_tp, proj_value, proj_gate, conv_saved, conv_taps, norm_gain, out_weight, cotangent):
+    fold = 2
+    n_z = n_sp // fold
+    rows, width = cotangent.shape
+    ch = conv_saved.shape[1]
+    n_taps = conv_taps.shape[0]
+    part = width // n_sp
+    dma = pltpu.SemaphoreType.DMA
+    V = pltpu.VMEM
+    bf = jnp.bfloat16
+    vm = pl.BlockSpec(memory_space=pltpu.VMEM)
+    return pl.pallas_call(
+        functools.partial(kernel, n_sp, n_tp, fold),
+        out_shape=(
+            jax.ShapeDtypeStruct((rows, ch), bf),
+            jax.ShapeDtypeStruct((rows, ch), bf),
+            jax.ShapeDtypeStruct((ch, part), f32),
+            jax.ShapeDtypeStruct((n_taps, ch), f32),
+        ),
+        in_specs=[vm] * 7,
+        out_specs=[vm] * 4,
+        scratch_shapes=[
+            V((ch, rows), bf), V((rows, ch), f32), V((rows + 32, ch), f32), V((8, rows + 32, ch), f32),
+            V((rows, 128), f32), V((rows, 128), f32),
+            V((n_sp, ch, part), f32), V((n_z, ch, part), f32), V((n_z, ch, part), f32),
+            V((n_z, ch, part), f32),
+            V((8, rows), f32), V((n_tp - 1, 8, rows), f32), V((8, rows), f32), V((n_tp - 1, 8, rows), f32),
+            V((n_taps, 8, ch), f32), V((32, ch), f32), V((32, ch), f32), V((n_z - 1, 32, ch), f32),
+            V((32, ch), f32), V((n_taps, 8, ch), f32),
+            dma((n_tp - 1,)), dma((n_tp - 1,)), dma((n_tp - 1,)), dma((n_tp - 1,)),
+            dma((n_z,)), dma((n_z,)), dma((n_z,)), dma((n_z,)), dma((n_z,)), dma((n_z,)),
+            dma, dma, dma((n_z - 1,)), dma((n_z - 1,)), dma, dma,
+        ],
+        compiler_params=pltpu.CompilerParams(
+            collective_id=0, has_side_effects=True, vmem_limit_bytes=60 * 1024 * 1024
+        ),
+    )(proj_value, proj_gate, conv_saved, conv_taps, norm_gain.reshape(1, ch), out_weight, cotangent)
 
 
 def passed_along(block, axis, distance):
@@ -72,4 +449,14 @@
         P("sp", None),
     )
     out_specs = (P("sp", "tp"), P("sp", "tp"), P("tp", "sp"), P(None, "tp"))
-    return jax.shard_map(local, mesh=mesh, in_specs=in_specs, out_specs=out_specs, check_vma=False)
+    n_sp, n_tp = mesh.shape["sp"], mesh.shape["tp"]
+
+    def step(*args):
+        rows, width = args[6].shape
+        ch, n_taps = args[2].shape[1], args[3].shape[0]
+        small = n_sp % 2 == 0 and 4 <= n_sp <= 8 and width % n_sp == 0 and n_tp > 1
+        if small and rows % 128 == 0 and rows >= 128 and ch % 8 == 0 and 24 < n_taps <= 31:
+            return fused(n_sp, n_tp, *args)
+        return local(*args)
+
+    return jax.shard_map(step, mesh=mesh, in_specs=in_specs, out_specs=out_specs, check_vma=False)

time: 201 us -> 89.6 us (0.45); the launches traced: 198 us -> 89.2 us
  waiting for transfers between devices: 86.4 us -> 0 us
  Pallas kernels: 0 us -> 73 us
  blocking collectives: 42.8 us -> 0 us
  other arithmetic: 41.3 us -> 0 us
  between operations: 14.8 us -> 0.67 us
  local copies, waits for them, and re-layouts: 2.27 us -> 15.6 us
  matrix products: 7.72 us -> 0 us
  starting transfers between devices: 2.62 us -> 0 us
    unnamed x2 -> x0, waiting for transfers between devices: 83.8 us -> none
    pallas_call x0 -> x1, Pallas kernels: none -> 73 us  [fused(): pl.pallas_call(functools.partial(kernel, n_sp, n_tp, fold), out_shape=(ja...]
    psum x3 -> x0, blocking collectives: 42.8 us -> none  [the longest x1 30.1 us: local(): grad_taps = lax.psum(jnp.stack(tap_rows), 'sp') * grad_scale]
    reduce_sum x5 -> x0, other arithmetic: 18.5 us -> none  [the longest x4 17.2 us: local(): tap_rows.append(jnp.sum(gated * shifted, axis=0))]
    convert_element_type x2 -> x0, other arithmetic: 18.3 us -> none  [the longest x1 17.6 us: local(): grad_gate = (d_glu * gated * (1.0 - gate_proj)).astype(jnp.bfloat16)]
    unnamed x13 -> x12, local copies, waits for them, and re-layouts: 1.34 us -> 10 us
    dot_general x2 -> x0, matrix products: 7.72 us -> none  [the longest x1 4.27 us: local(): lax.dot_general(cotangent, out_weight, (((1,), (1,)), ((), ())), preferre...]
    mul x3 -> x0, other arithmetic: 4.43 us -> none  [the longest x1 2.12 us: local(): grad_out_weight = shard_grad.T * grad_scale]
  transfers between devices with their start and end apart: 2 -> 0, of which waited for: 2 -> 0; matrix products, arithmetic and copies ran while one was open for 20% -> 0% of each run, Pallas kernels for 0% -> 0%
where the time goes in v1:
time: 89.6 us; the launch traced here: 89.2 us
  Pallas kernels  73 us (81%)
  local copies, waits for them, and re-layouts  15.6 us (17%)
    pallas_call x1, Pallas kernels, fused(): pl.pallas_call(functools.partial(kernel, n_sp, n_tp, fold), out_shape=(ja...  73 us
    unnamed x12, local copies, waits for them, and re-layouts  10 us
    pallas_call x2, local copies, waits for them, and re-layouts, fused(): pl.pallas_call(functools.partial(kernel, n_sp, n_tp, fold), out_shape=(ja...  4.13 us

profile of v1, /device:TPU:12, one launch (start us, length us, event | category | flops | bytes accessed | tf_op | source)
XLA Modules:
  0.0 89.2 jit_solution(672926108137643935)
XLA Ops:
  0.6 0.0 copy-start
  0.6 1.4 %reshape.11.gain = bf16[1,504]{1,0:T(2,128)(2,1)} reshape(bf16[504]{0:T(512)(128)(2,1)} %param.11) | data formatting | bytes 2016 | tf_op jit(solution)/shard_map/reshape | solution.py:385
  2.0 2.0 %copy.11.pv = bf16[512,504]{1,0:T(8,128)(2,1)} copy(bf16[512,504]{0,1:T(8,128)(2,1)} %param.7) | data formatting | bytes 1032192 | tf_op args[0]
  4.1 2.1 %copy.12.pg = bf16[512,504]{1,0:T(8,128)(2,1)} copy(bf16[512,504]{0,1:T(8,128)(2,1)} %param.8) | data formatting | bytes 1032192 | tf_op args[1]
  6.1 2.0 %copy.13.conv = bf16[512,504]{1,0:T(8,128)(2,1)} copy(bf16[512,504]{0,1:T(8,128)(2,1)} %param.9) | data formatting | bytes 1032192 | tf_op args[2]
  8.2 0.0 copy-done
  8.2 2.5 %copy.14.cot = bf16[512,2016]{1,0:T(8,128)(2,1)} copy(bf16[512,2016]{0,1:T(8,128)(2,1)S(1)} %copy-done) | data formatting | bytes 4128768 | tf_op args[6]
  10.7 73.0 %shard_map.102 = (bf16[512,504]{1,0:T(8,128)(2,1)}, bf16[512,504]{1,0:T(8,128)(2,1)}, f32[504,252]{1,0:T(8,128)}, f32[31,504]{1,0:T(8,128)}) custom-call(bf16[512,504]{1,0:T(8,128)(2,1)} %copy.11.pv, bf16[512,504]{1,0:T(8,128)(2,1)} %copy.12.pg, bf16[512,504]{1,0:T(8,128)(2,1)} %copy.13.conv, bf16[31,504]{1,0:T(8,128)(2,1)} %taps.1, ...), custom_call_target="tpu_custom_call" | custom-call | tf_op jit(solution)/shard_map/pallas_call | solution.py:360
  83.7 0.0 copy-start.1
  83.7 0.0 copy-start.2
  83.7 2.1 %copy.15 = bf16[512,504]{0,1:T(8,128)(2,1)} copy(bf16[512,504]{1,0:T(8,128)(2,1)} %get-tuple-element.4) | data formatting | bytes 1032192 | tf_op jit(solution)/shard_map/pallas_call | solution.py:360
  85.8 2.0 %copy.16 = bf16[512,504]{0,1:T(8,128)(2,1)} copy(bf16[512,504]{1,0:T(8,128)(2,1)} %get-tuple-element.5) | data formatting | bytes 1032192 | tf_op jit(solution)/shard_map/pallas_call | solution.py:360
  87.8 0.0 copy-done.1
  87.8 0.8 copy.19
  88.6 0.0 copy-done.2
  88.6 0.6 copy.20
Async XLA Ops:
  0.6 7.6 %copy-start = (bf16[512,2016]{0,1:T(8,128)(2,1)S(1)}, bf16[512,2016]{0,1:T(8,128)(2,1)}, u32[]{:S(2)}) copy-start(bf16[512,2016]{0,1:T(8,128)(2,1)} %param.13) | copy-start | bytes 6193156
  83.7 4.2 %copy-start.1 = (f32[504,252]{1,0:T(8,128)S(1)}, f32[504,252]{1,0:T(8,128)}, u32[]{:S(2)}) copy-start(f32[504,252]{1,0:T(8,128)} %get-tuple-element.14) | copy-start | bytes 1524100
  83.7 4.9 %copy-start.2 = (f32[31,504]{1,0:T(8,128)S(1)}, f32[31,504]{1,0:T(8,128)}, u32[]{:S(2)}) copy-start(f32[31,504]{1,0:T(8,128)} %get-tuple-element.15) | copy-start | bytes 187492

commit v2 on v1

--- a/solution.py
+++ b/solution.py
@@ -29,9 +29,9 @@
 
 
 def kernel(
-    n_sp, n_tp, fold, pv, pg, conv, taps, gain, weight, cot,
+    n_sp, n_tp, fold, pv_h, pg_h, conv, taps, gain, weight_h, cot_h,
     out_v, out_g, out_w, out_t,
-    act_t, d_act, ext, shifted, cols, cols2, term, got_y, got_r, got_l,
+    pv, pg, weight, cot, in_sems, gain_c, gated_s, d_glu_s, act_t, d_act, ext, shifted, cols, cols2, term, got_y, got_r, got_l,
     stat, stat_in, mom, mom_in, grad_acc, g_own, g_mid, g_in, g_yin, taps_b,
     stat_ss, stat_rs, mom_ss, mom_rs, y_ss, y_rs, r_ss, r_rs, l_ss, l_rs,
     halo_ss, halo_rs, gz_ss, gz_rs, gy_ss, gy_rs,
@@ -42,32 +42,36 @@
     z = s // fold
     y = s % fold
     other_y = 1 - y
-    rows, width = cot.shape
-    ch = conv.shape[1]
+    width, rows = cot.shape
+    ch = conv.shape[0]
     part = out_w.shape[1]
     n_taps = taps.shape[0]
     scale = 1.0 / math.sqrt(rows * n_sp)
     blk = 128
     n_blk = rows // blk
 
+    loads = [
+        pltpu.make_async_copy(a, b, in_sems.at[i])
+        for i, (a, b) in enumerate([(cot_h, cot), (weight_h, weight), (pv_h, pv), (pg_h, pg)])
+    ]
+    for c in loads:
+        c.start()
+
     barrier = pltpu.get_barrier_semaphore()
     for i in range(1, n_sp):
         pl.semaphore_signal(barrier, inc=1, device_id=(lax.rem(s + i, n_sp), t), device_id_type=MESH)
     for i in range(1, n_tp):
         pl.semaphore_signal(barrier, inc=1, device_id=(s, lax.rem(t + i, n_tp)), device_id_type=MESH)
 
-    def pack(a, b):
-        lane = lax.broadcasted_iota(jnp.int32, (blk, blk), 1)
-        return jnp.where(lane == 0, a, b).T[:8]
-
-    def unpack(x):
-        return jnp.concatenate([x] * (blk // 8), axis=0).T
-
-    @pl.loop(0, n_blk)
-    def _(i):
-        at = pl.ds(pl.multiple_of(i * blk, blk), blk)
-        c = conv[at, :].astype(f32)
-        stat[:, at] = pack(jnp.sum(c, axis=1, keepdims=True), jnp.sum(c * c, axis=1, keepdims=True))
+    row8b = lax.broadcasted_iota(jnp.int32, (8, blk), 0)
+
+    @pl.loop(0, n_blk)
+    def _(i):
+        at = pl.ds(pl.multiple_of(i * blk, blk), blk)
+        c = conv[:, at].astype(f32)
+        stat[:, at] = jnp.where(
+            row8b == 0, jnp.sum(c, axis=0, keepdims=True), jnp.sum(c * c, axis=0, keepdims=True)
+        )
 
     pl.semaphore_wait(barrier, n_sp - 1 + n_tp - 1)
 
@@ -84,12 +88,15 @@
     for c in stat_copies:
         c.start()
 
-    @pl.loop(0, n_blk)
-    def _(i):
-        at = pl.ds(pl.multiple_of(i * blk, blk), blk)
-        d_act[at, :] = lax.dot_general(
-            cot[at, :], weight[...], (((1,), (1,)), ((), ())), preferred_element_type=f32
-        )
+    gain_c[...] = jnp.broadcast_to(gain[...].astype(f32), (128, ch)).T
+    loads[0].wait()
+    loads[1].wait()
+    wide_blk = 256 if rows % 256 == 0 else 128
+
+    @pl.loop(0, rows // wide_blk)
+    def _(i):
+        at = pl.ds(pl.multiple_of(i * wide_blk, wide_blk), wide_blk)
+        d_act[:, at] = jnp.dot(weight[...], cot[:, at], preferred_element_type=f32)
 
     for c in stat_copies:
         c.wait()
@@ -99,22 +106,20 @@
     mean = total[0:1] / width
     inv = lax.rsqrt(total[1:2] / width - mean * mean + norm_eps)
     row8 = lax.broadcasted_iota(jnp.int32, (8, rows), 0)
-    both = jnp.where(row8 == 0, mean, inv)
-    for i in range(n_blk):
-        cols[i * blk:(i + 1) * blk, :] = unpack(both[:, i * blk:(i + 1) * blk])
-
-    gain_f = gain[...].astype(f32)
-
-    @pl.loop(0, n_blk)
-    def _(i):
-        at = pl.ds(pl.multiple_of(i * blk, blk), blk)
-        c = conv[at, :].astype(f32)
-        normed = (c - cols[at, 0:1]) * cols[at, 1:2] * gain_f
-        a = normed * jax.nn.sigmoid(normed)
-        act_t[:, at] = a.T.astype(jnp.bfloat16)
+    cols[...] = jnp.where(row8 == 0, mean, inv)
+
+    @pl.loop(0, n_blk)
+    def _(i):
+        at = pl.ds(pl.multiple_of(i * blk, blk), blk)
+        c = conv[:, at].astype(f32)
+        normed = (c - cols[0:1, at]) * cols[1:2, at] * gain_c[...]
+        act_t[:, at] = (normed * jax.nn.sigmoid(normed)).astype(jnp.bfloat16)
 
     for j in range(n_sp):
-        term[j] = jnp.dot(act_t[...], cot[:, j * part:(j + 1) * part], preferred_element_type=f32)
+        term[j] = lax.dot_general(
+            act_t[...], cot[j * part:(j + 1) * part, :], (((1,), (1,)), ((), ())),
+            preferred_element_type=f32,
+        )
 
     orders = line_order(n_z)
     dest = [lookup([orders[i][k] for i in range(n_z)], z) for k in range(n_z)]
@@ -175,14 +180,15 @@
     @pl.loop(0, n_blk)
     def _(i):
         at = pl.ds(pl.multiple_of(i * blk, blk), blk)
-        c = conv[at, :].astype(f32)
-        centered = (c - cols[at, 0:1]) * cols[at, 1:2]
-        normed = centered * gain_f
+        c = conv[:, at].astype(f32)
+        centered = (c - cols[0:1, at]) * cols[1:2, at]
+        normed = centered * gain_c[...]
         gate = jax.nn.sigmoid(normed)
-        d_hat = d_act[at, :] * gate * (1.0 + normed * (1.0 - gate)) * gain_f
-        d_act[at, :] = d_hat
-        mom[:, at] = pack(
-            jnp.sum(d_hat, axis=1, keepdims=True), jnp.sum(d_hat * centered, axis=1, keepdims=True)
+        d_hat = d_act[:, at] * gate * (1.0 + normed * (1.0 - gate)) * gain_c[...]
+        d_act[:, at] = d_hat
+        mom[:, at] = jnp.where(
+            row8b == 0, jnp.sum(d_hat, axis=0, keepdims=True),
+            jnp.sum(d_hat * centered, axis=0, keepdims=True),
         )
 
     mom_copies = tp_copies(mom, mom_in, mom_ss, mom_rs)
@@ -191,22 +197,28 @@
     for k in range(n_taps):
         taps_b[k] = jnp.broadcast_to(taps[k:k + 1, :].astype(f32), (8, ch))
     grad_acc[...] = jnp.zeros_like(grad_acc)
+    loads[2].wait()
+    loads[3].wait()
+
+    @pl.loop(0, n_blk)
+    def _(i):
+        at = pl.ds(pl.multiple_of(i * blk, blk), blk)
+        gated_s[at, :] = (pv[:, at].astype(f32) * jax.nn.sigmoid(pg[:, at].astype(f32))).T
+
     for c in mom_copies:
         c.wait()
     total = mom[...]
     for i in range(n_tp - 1):
         total = total + mom_in[i]
-    total = total / width
-    for i in range(n_blk):
-        cols2[i * blk:(i + 1) * blk, :] = unpack(total[:, i * blk:(i + 1) * blk])
-
-    @pl.loop(0, n_blk)
-    def _(i):
-        at = pl.ds(pl.multiple_of(i * blk, blk), blk)
-        c = conv[at, :].astype(f32)
-        inv_std = cols[at, 1:2]
-        centered = (c - cols[at, 0:1]) * inv_std
-        ext[at, :] = inv_std * (d_act[at, :] - cols2[at, 0:1] - centered * cols2[at, 1:2])
+    cols2[...] = total / width
+
+    @pl.loop(0, n_blk)
+    def _(i):
+        at = pl.ds(pl.multiple_of(i * blk, blk), blk)
+        c = conv[:, at].astype(f32)
+        inv_std = cols[1:2, at]
+        centered = (c - cols[0:1, at]) * inv_std
+        ext[at, :] = (inv_std * (d_act[:, at] - cols2[0:1, at] - centered * cols2[1:2, at])).T
 
     reach = 32
     back = jnp.maximum(s - 1, 0)
@@ -237,8 +249,7 @@
             def body(i, accs):
                 start = pl.multiple_of(i * reach, reach)
                 at = pl.ds(start, reach)
-                gate = jax.nn.sigmoid(pg[at, ln].astype(f32))
-                gated = pv[at, ln].astype(f32) * gate
+                gated = gated_s[at, ln]
                 d_glu = jnp.zeros((reach, wide), f32)
                 out = []
                 for o in range(n_taps):
@@ -250,8 +261,7 @@
                     for q in range(reach // 8):
                         acc = acc + prod[8 * q:8 * q + 8]
                     out.append(acc)
-                out_v[at, ln] = (d_glu * gate).astype(jnp.bfloat16)
-                out_g[at, ln] = (d_glu * gated * (1.0 - gate)).astype(jnp.bfloat16)
+                d_glu_s[at, ln] = d_glu
                 return tuple(out)
 
             accs = tuple(grad_acc[n_taps - 1 - o, :, ln] for o in range(n_taps))
@@ -300,6 +310,15 @@
         c.start()
     for k in range(2, n_z - 1):
         hop(k)
+
+    @pl.loop(0, n_blk)
+    def _(i):
+        at = pl.ds(pl.multiple_of(i * blk, blk), blk)
+        gate = jax.nn.sigmoid(pg[:, at].astype(f32))
+        d_glu = d_glu_s[at, :].T
+        out_v[:, at] = (d_glu * gate).astype(jnp.bfloat16)
+        out_g[:, at] = (d_glu * (pv[:, at].astype(f32) * gate) * (1.0 - gate)).astype(jnp.bfloat16)
+
     for c in gz_copies:
         c.wait()
     total = g_own[...]
@@ -357,19 +376,22 @@
     V = pltpu.VMEM
     bf = jnp.bfloat16
     vm = pl.BlockSpec(memory_space=pltpu.VMEM)
-    return pl.pallas_call(
+    hb = pl.BlockSpec(memory_space=pl.ANY)
+    grad_value, grad_gate, grad_weight, grad_taps = pl.pallas_call(
         functools.partial(kernel, n_sp, n_tp, fold),
         out_shape=(
-            jax.ShapeDtypeStruct((rows, ch), bf),
-            jax.ShapeDtypeStruct((rows, ch), bf),
+            jax.ShapeDtypeStruct((ch, rows), bf),
+            jax.ShapeDtypeStruct((ch, rows), bf),
             jax.ShapeDtypeStruct((ch, part), f32),
             jax.ShapeDtypeStruct((n_taps, ch), f32),
         ),
-        in_specs=[vm] * 7,
+        in_specs=[hb, hb, vm, vm, vm, hb, hb],
         out_specs=[vm] * 4,
         scratch_shapes=[
-            V((ch, rows), bf), V((rows, ch), f32), V((rows + 32, ch), f32), V((8, rows + 32, ch), f32),
-            V((rows, 128), f32), V((rows, 128), f32),
+            V((ch, rows), bf), V((ch, rows), bf), V((ch, width), bf), V((width, rows), bf), dma((4,)),
+            V((ch, 128), f32), V((rows, ch), f32), V((rows, ch), f32),
+            V((ch, rows), bf), V((ch, rows), f32), V((rows + 32, ch), f32), V((8, rows + 32, ch), f32),
+            V((8, rows), f32), V((8, rows), f32),
             V((n_sp, ch, part), f32), V((n_z, ch, part), f32), V((n_z, ch, part), f32),
             V((n_z, ch, part), f32),
             V((8, rows), f32), V((n_tp - 1, 8, rows), f32), V((8, rows), f32), V((n_tp - 1, 8, rows), f32),
@@ -382,7 +404,11 @@
         compiler_params=pltpu.CompilerParams(
             collective_id=0, has_side_effects=True, vmem_limit_bytes=60 * 1024 * 1024
         ),
-    )(proj_value, proj_gate, conv_saved, conv_taps, norm_gain.reshape(1, ch), out_weight, cotangent)
+    )(
+        proj_value.T, proj_gate.T, conv_saved.T, conv_taps, norm_gain.reshape(1, ch), out_weight,
+        cotangent.T,
+    )
+    return grad_value.T, grad_gate.T, grad_weight, grad_taps
 
 
 def passed_along(block, axis, distance):

time: 89.6 us -> 76.5 us (0.85)
  local copies, waits for them, and re-layouts: 15.6 us -> 6.46 us
  Pallas kernels: 73 us -> 69.2 us
    unnamed x12 -> x8, local copies, waits for them, and re-layouts: 10 us -> 5.2 us
    pallas_call x2 -> x0, local copies, waits for them, and re-layouts: 4.13 us -> none  [fused(): pl.pallas_call(functools.partial(kernel, n_sp, n_tp, fold), out_shape=(ja...]
    pallas_call x1, Pallas kernels: 73 us -> 69.2 us  [fused(): pl.pallas_call(functools.partial(kernel, n_sp, n_tp, fold), out_shape=(ja...]
where the time goes in v2:
time: 76.5 us; the launch traced here: 76.3 us
  Pallas kernels  69.2 us (90%)
  local copies, waits for them, and re-layouts  6.46 us (8%)
    pallas_call x1, Pallas kernels, fused(): pl.pallas_call(functools.partial(kernel, n_sp, n_tp, fold), out_shape=(ja...  69.2 us
    unnamed x8, local copies, waits for them, and re-layouts  5.2 us

profile of v2, /device:TPU:12, one launch (start us, length us, event | category | flops | bytes accessed | tf_op | source)
XLA Modules:
  0.0 76.3 jit_solution(6919369492499412514)
XLA Ops:
  0.6 1.3 %reshape.11.gain = bf16[1,504]{1,0:T(2,128)(2,1)} reshape(bf16[504]{0:T(512)(128)(2,1)} %param.11) | data formatting | bytes 2016 | tf_op jit(solution)/shard_map/reshape | solution.py:408
  1.9 69.2 %shard_map.102 = (bf16[504,512]{1,0:T(8,128)(2,1)}, bf16[504,512]{1,0:T(8,128)(2,1)}, f32[504,252]{1,0:T(8,128)}, f32[31,504]{1,0:T(8,128)}) custom-call(bf16[504,512]{1,0:T(8,128)(2,1)} %bitcast.9, bf16[504,512]{1,0:T(8,128)(2,1)} %bitcast.10, bf16[504,512]{1,0:T(8,128)(2,1)} %bitcast.11, bf16[31,504]{1,0:T(8,128)(2,1)} %taps.1, ...), custom_call_target="tpu_custom_call" | custom-call | tf_op jit(solution)/shard_map/pallas_call | solution.py:380
  71.1 0.0 copy-start
  71.1 0.0 copy-start.1
  71.1 1.9 %copy.15 = bf16[512,504]{0,1:T(8,128)(2,1)} copy(bf16[512,504]{0,1:T(8,128)(2,1)} %bitcast.8) | data formatting | bytes 1032192
  73.0 1.9 %copy.16 = bf16[512,504]{0,1:T(8,128)(2,1)} copy(bf16[512,504]{0,1:T(8,128)(2,1)} %bitcast.7) | data formatting | bytes 1032192
  74.9 0.0 copy-done
  74.9 0.8 %copy.17 = f32[504,252]{1,0:T(8,128)} copy(f32[504,252]{1,0:T(8,128)S(1)} %copy-done) | data formatting | bytes 1016064
  75.7 0.0 copy-done.1
  75.7 0.6 copy.18
Async XLA Ops:
  71.1 3.8 %copy-start = (f32[504,252]{1,0:T(8,128)S(1)}, f32[504,252]{1,0:T(8,128)}, u32[]{:S(2)}) copy-start(f32[504,252]{1,0:T(8,128)} %get-tuple-element.18) | copy-start | bytes 1524100
  71.1 4.6 %copy-start.1 = (f32[31,504]{1,0:T(8,128)S(1)}, f32[31,504]{1,0:T(8,128)}, u32[]{:S(2)}) copy-start(f32[31,504]{1,0:T(8,128)} %get-tuple-element.19) | copy-start | bytes 187492

commit v3 on v2

--- a/solution.py
+++ b/solution.py
@@ -21,6 +21,10 @@
     return rows
 
 
+def low_rows(ch):
+    return max(ch // 7 // 8 * 8, 8)
+
+
 def lookup(table, place):
     value = table[0]
     for i in range(1, len(table)):
@@ -28,12 +32,26 @@
     return value
 
 
+def finish(v_in, g_in, w_in, t_in, v_out, g_out, w_out, t_out, v_b, g_b, w_b, t_b, ss):
+    trips = [(v_in, v_b, v_out), (g_in, g_b, g_out), (w_in, w_b, w_out), (t_in, t_b, t_out)]
+    inward = [pltpu.make_async_copy(a, b, ss.at[i]) for i, (a, b, _) in enumerate(trips)]
+    outward = [pltpu.make_async_copy(b, c, ss.at[4 + i]) for i, (_, b, c) in enumerate(trips)]
+    for c in inward:
+        c.start()
+    for a, b in zip(inward, outward):
+        a.wait()
+        b.start()
+    for b in outward:
+        b.wait()
+
+
 def kernel(
     n_sp, n_tp, fold, pv_h, pg_h, conv, taps, gain, weight_h, cot_h,
     out_v, out_g, out_w, out_t,
-    pv, pg, weight, cot, in_sems, gain_c, gated_s, d_glu_s, act_t, d_act, ext, shifted, cols, cols2, term, got_y, got_r, got_l,
+    pv, pg, weight, cot, in_sems, gain_c, gated_s, d_glu_s, act_t, d_act, ext, shifted, cols, cols2, term, got_y, got_r, got_l, low_r, low_l, low_y,
     stat, stat_in, mom, mom_in, grad_acc, g_own, g_mid, g_in, g_yin, taps_b,
     stat_ss, stat_rs, mom_ss, mom_rs, y_ss, y_rs, r_ss, r_rs, l_ss, l_rs,
+    lr_ss, lr_rs, ll_ss, ll_rs, ly_ss, ly_rs,
     halo_ss, halo_rs, gz_ss, gz_rs, gy_ss, gy_rs,
 ):
     s = lax.axis_index("sp")
@@ -49,6 +67,8 @@
     scale = 1.0 / math.sqrt(rows * n_sp)
     blk = 128
     n_blk = rows // blk
+    low = low_rows(ch)
+    top = ch - low
 
     loads = [
         pltpu.make_async_copy(a, b, in_sems.at[i])
@@ -88,7 +108,7 @@
     for c in stat_copies:
         c.start()
 
-    gain_c[...] = jnp.broadcast_to(gain[...].astype(f32), (128, ch)).T
+    gain_c[...] = jnp.broadcast_to(gain[...].astype(f32).reshape(1, ch), (128, ch)).T
     loads[0].wait()
     loads[1].wait()
     wide_blk = 256 if rows % 256 == 0 else 128
@@ -126,7 +146,7 @@
 
     def y_copy(k):
         return pltpu.make_async_remote_copy(
-            src_ref=term.at[dest[k] * fold + other_y], dst_ref=got_y.at[dest[k]],
+            src_ref=term.at[dest[k] * fold + other_y, pl.ds(0, top), :], dst_ref=got_y.at[dest[k]],
             send_sem=y_ss.at[dest[k]], recv_sem=y_rs.at[dest[k]],
             device_id=(z * fold + other_y, t), device_id_type=MESH,
         )
@@ -138,15 +158,15 @@
         to = z + 1 if up else z - 1
         to = jnp.clip(to, 0, n_z - 1)
         return pltpu.make_async_remote_copy(
-            src_ref=term.at[d * fold + y], dst_ref=buf.at[d], send_sem=ss.at[d], recv_sem=rs.at[d],
+            src_ref=term.at[d * fold + y, pl.ds(0, top), :], dst_ref=buf.at[d], send_sem=ss.at[d], recv_sem=rs.at[d],
             device_id=(to * fold + y, t), device_id_type=MESH,
         )
 
     def add_into(d, buf):
         own = d * fold + y
-        step = 56 if ch % 56 == 0 else 8
-
-        @pl.loop(0, ch // step)
+        step = max(c for c in range(8, 65, 8) if top % c == 0)
+
+        @pl.loop(0, top // step)
         def _(i):
             at = pl.ds(pl.multiple_of(i * step, 8), step)
             term[own, at, :] = term[own, at, :] + buf[d, at, :]
@@ -174,8 +194,62 @@
 
             line_copy(d, False).start()
 
+    def low_copy(d, up):
+        buf, ss, rs = (low_r, lr_ss, lr_rs) if up else (low_l, ll_ss, ll_rs)
+        to = jnp.clip(z + 1 if up else z - 1, 0, n_z - 1)
+        return pltpu.make_async_remote_copy(
+            src_ref=term.at[pl.ds(d * fold, fold), pl.ds(top, low), :], dst_ref=buf.at[d],
+            send_sem=ss.at[d], recv_sem=rs.at[d], device_id=(to * fold + y, t), device_id_type=MESH,
+        )
+
+    def low_take(d, up):
+        low_copy(d, up).wait_recv()
+        buf = low_r if up else low_l
+        at = pl.ds(d * fold, fold)
+        term[at, pl.ds(top, low), :] = term[at, pl.ds(top, low), :] + buf[d]
+
+    def low_hop(k):
+        d = dest[k]
+
+        @pl.when(d > z)
+        def _():
+            @pl.when(z > 0)
+            def _():
+                low_take(d, True)
+
+            low_copy(d, True).start()
+
+        @pl.when(d < z)
+        def _():
+            @pl.when(z < n_z - 1)
+            def _():
+                low_take(d, False)
+
+            low_copy(d, False).start()
+
+    low_swap = pltpu.make_async_remote_copy(
+        src_ref=term.at[z * fold + other_y, pl.ds(top, low), :], dst_ref=low_y,
+        send_sem=ly_ss, recv_sem=ly_rs, device_id=(z * fold + other_y, t), device_id_type=MESH,
+    )
+
+    def low_end():
+        @pl.when(z > 0)
+        def _():
+            low_take(z, True)
+
+        @pl.when(z < n_z - 1)
+        def _():
+            low_take(z, False)
+
+        low_swap.start()
+
     y_copies[0].start()
     y_copies[1].start()
+
+    @pl.when(jnp.logical_or(z == 0, z == n_z - 1))
+    def _():
+        for k in range(n_z - 1):
+            low_hop(k)
 
     @pl.loop(0, n_blk)
     def _(i):
@@ -191,6 +265,7 @@
             jnp.sum(d_hat * centered, axis=0, keepdims=True),
         )
 
+    mid = jnp.logical_and(z > 0, z < n_z - 1)
     mom_copies = tp_copies(mom, mom_in, mom_ss, mom_rs)
     for c in mom_copies:
         c.start()
@@ -271,11 +346,18 @@
 
     n_row = rows // reach
 
+    @pl.when(mid)
+    def _():
+        for k in range(n_z - 1):
+            low_hop(k)
+
+
     @pl.loop(0, n_row - 1)
     def _(i):
         shift_block(i)
 
     hop(0)
+    low_end()
     half = (n_row - 2) // 2
     conv_blocks(0, half)
     hop(1)
@@ -343,7 +425,10 @@
         line_copy(z, False).wait_recv()
         add_into(z, got_l)
 
-    out_w[...] = term[z * fold + y] * scale
+    low_swap.wait()
+    own = z * fold + y
+    out_w[:top, :] = term[own, :top, :] * scale
+    out_w[top:, :] = (term[own, top:, :] + low_y[...]) * scale
     gy.wait()
     out_t[...] = ((g_mid[...] + g_yin[...]) * scale)[:n_taps]
     for k in range(n_z):
@@ -359,10 +444,12 @@
         @pl.when(d > z)
         def _():
             line_copy(d, True).wait_send()
+            low_copy(d, True).wait_send()
 
         @pl.when(d < z)
         def _():
             line_copy(d, False).wait_send()
+            low_copy(d, False).wait_send()
 
 
 def fused(n_sp, n_tp, proj_value, proj_gate, conv_saved, conv_taps, norm_gain, out_weight, cotangent):
@@ -372,6 +459,8 @@
     ch = conv_saved.shape[1]
     n_taps = conv_taps.shape[0]
     part = width // n_sp
+    low = low_rows(ch)
+    top = ch - low
     dma = pltpu.SemaphoreType.DMA
     V = pltpu.VMEM
     bf = jnp.bfloat16
@@ -392,22 +481,33 @@
             V((ch, 128), f32), V((rows, ch), f32), V((rows, ch), f32),
             V((ch, rows), bf), V((ch, rows), f32), V((rows + 32, ch), f32), V((8, rows + 32, ch), f32),
             V((8, rows), f32), V((8, rows), f32),
-            V((n_sp, ch, part), f32), V((n_z, ch, part), f32), V((n_z, ch, part), f32),
-            V((n_z, ch, part), f32),
+            V((n_sp, ch, part), f32), V((n_z, top, part), f32), V((n_z, top, part), f32),
+            V((n_z, top, part), f32),
+            V((n_z, fold, low, part), f32), V((n_z, fold, low, part), f32), V((low, part), f32),
             V((8, rows), f32), V((n_tp - 1, 8, rows), f32), V((8, rows), f32), V((n_tp - 1, 8, rows), f32),
             V((n_taps, 8, ch), f32), V((32, ch), f32), V((32, ch), f32), V((n_z - 1, 32, ch), f32),
             V((32, ch), f32), V((n_taps, 8, ch), f32),
             dma((n_tp - 1,)), dma((n_tp - 1,)), dma((n_tp - 1,)), dma((n_tp - 1,)),
             dma((n_z,)), dma((n_z,)), dma((n_z,)), dma((n_z,)), dma((n_z,)), dma((n_z,)),
+            dma((n_z,)), dma((n_z,)), dma((n_z,)), dma((n_z,)), dma, dma,
             dma, dma, dma((n_z - 1,)), dma((n_z - 1,)), dma, dma,
         ],
         compiler_params=pltpu.CompilerParams(
             collective_id=0, has_side_effects=True, vmem_limit_bytes=60 * 1024 * 1024
         ),
     )(
-        proj_value.T, proj_gate.T, conv_saved.T, conv_taps, norm_gain.reshape(1, ch), out_weight,
+        proj_value.T, proj_gate.T, conv_saved.T, conv_taps, norm_gain, out_weight,
         cotangent.T,
     )
+    results = (grad_value, grad_gate, grad_weight, grad_taps)
+    grad_value, grad_gate, grad_weight, grad_taps = pl.pallas_call(
+        finish,
+        out_shape=tuple(jax.ShapeDtypeStruct(r.shape, r.dtype) for r in results),
+        in_specs=[hb] * 4,
+        out_specs=[hb] * 4,
+        scratch_shapes=[V(r.shape, r.dtype) for r in results] + [dma((8,))],
+        compiler_params=pltpu.CompilerParams(vmem_limit_bytes=60 * 1024 * 1024),
+    )(*results)
     return grad_value.T, grad_gate.T, grad_weight, grad_taps
 
 

time: 76.5 us -> 64 us (0.84)
  local copies, waits for them, and re-layouts: 6.46 us -> 0 us
  Pallas kernels: 69.2 us -> 63.1 us
    pallas_call x1, Pallas kernels: 69.2 us -> 60.8 us  [fused(): pl.pallas_call(functools.partial(kernel, n_sp, n_tp, fold), out_shape=(ja...]
    unnamed x8 -> x0, local copies, waits for them, and re-layouts: 5.2 us -> none
    pallas_call x0 -> x1, Pallas kernels: none -> 2.25 us  [fused(): pl.pallas_call(finish, out_shape=tuple((jax.ShapeDtypeStruct(r.shape, r.d...]
    reshape x1 -> x0, local copies, waits for them, and re-layouts: 1.26 us -> none  [fused(): norm_gain.reshape(1, ch)]
where the time goes in v3:
time: 64 us; the launch traced here: 63.7 us
  Pallas kernels  63.1 us (99%)
  between operations  0.64 us (1%)
    pallas_call x1, Pallas kernels, fused(): pl.pallas_call(functools.partial(kernel, n_sp, n_tp, fold), out_shape=(ja...  60.8 us
    pallas_call x1, Pallas kernels, fused(): pl.pallas_call(finish, out_shape=tuple((jax.ShapeDtypeStruct(r.shape, r.d...  2.25 us

profile of v3, /device:TPU:12, one launch (start us, length us, event | category | flops | bytes accessed | tf_op | source)
XLA Modules:
  0.0 63.7 jit_solution(9273409528466457397)
XLA Ops:
  0.6 60.8 %shard_map.102 = (bf16[504,512]{1,0:T(8,128)(2,1)}, bf16[504,512]{1,0:T(8,128)(2,1)}, f32[504,252]{1,0:T(8,128)}, f32[31,504]{1,0:T(8,128)}) custom-call(bf16[504,512]{1,0:T(8,128)(2,1)} %bitcast.7, bf16[504,512]{1,0:T(8,128)(2,1)} %bitcast.8, bf16[504,512]{1,0:T(8,128)(2,1)} %bitcast.9, bf16[31,504]{1,0:T(8,128)(2,1)} %taps.1, bf16[504]{0:T(512)(128)(2,1)} %gain.1, ...), custom_call_target="tpu_custom_call" | custom-call | tf_op jit(solution)/shard_map/pallas_call | solution.py:469
  61.5 2.2 %shard_map.103 = (bf16[504,512]{1,0:T(8,128)(2,1)}, bf16[504,512]{1,0:T(8,128)(2,1)}, f32[504,252]{1,0:T(8,128)}, f32[31,504]{1,0:T(8,128)}) custom-call(bf16[504,512]{1,0:T(8,128)(2,1)} %get-tuple-element.12.v_in, bf16[504,512]{1,0:T(8,128)(2,1)} %get-tuple-element.13.g_in, f32[504,252]{1,0:T(8,128)} %get-tuple-element.14.w_in, ...), custom_call_target="tpu_custom_call" | custom-call | tf_op jit(solution)/shard_map/pallas_call | solution.py:503

commit v4 on v3

--- a/solution.py
+++ b/solution.py
@@ -135,64 +135,89 @@
         normed = (c - cols[0:1, at]) * cols[1:2, at] * gain_c[...]
         act_t[:, at] = (normed * jax.nn.sigmoid(normed)).astype(jnp.bfloat16)
 
-    for j in range(n_sp):
+    orders = line_order(n_z)
+    dest = [lookup([orders[i][k] for i in range(n_z)], z) for k in range(n_z)]
+
+    cut = top // 2 // 8 * 8
+    halves = [(0, cut), (cut, top - cut)]
+
+    def y_copy(k, h):
+        at = pl.ds(*halves[h])
+        sem = dest[k] * 2 + h
+        return pltpu.make_async_remote_copy(
+            src_ref=term.at[dest[k] * fold + other_y, at, :], dst_ref=got_y.at[dest[k], at, :],
+            send_sem=y_ss.at[sem], recv_sem=y_rs.at[sem],
+            device_id=(z * fold + other_y, t), device_id_type=MESH,
+        )
+
+    y_copies = [[y_copy(k, h) for h in range(2)] for k in range(n_z)]
+
+    def make_term(j):
         term[j] = lax.dot_general(
             act_t[...], cot[j * part:(j + 1) * part, :], (((1,), (1,)), ((), ())),
             preferred_element_type=f32,
         )
 
-    orders = line_order(n_z)
-    dest = [lookup([orders[i][k] for i in range(n_z)], z) for k in range(n_z)]
-
-    def y_copy(k):
-        return pltpu.make_async_remote_copy(
-            src_ref=term.at[dest[k] * fold + other_y, pl.ds(0, top), :], dst_ref=got_y.at[dest[k]],
-            send_sem=y_ss.at[dest[k]], recv_sem=y_rs.at[dest[k]],
-            device_id=(z * fold + other_y, t), device_id_type=MESH,
-        )
-
-    y_copies = [y_copy(k) for k in range(n_z)]
-
-    def line_copy(d, up):
+    lead = dest[0] * fold + other_y
+    leads = sorted({orders[i][0] * fold + o for i in range(n_z) for o in range(fold)})
+    for j in leads:
+        @pl.when(lead == j)
+        def _():
+            make_term(j)
+
+    for h in range(2):
+        y_copies[0][h].start()
+    for j in range(n_sp):
+        if j in leads:
+            @pl.when(lead != j)
+            def _():
+                make_term(j)
+        else:
+            make_term(j)
+
+
+    def line_copy(d, h, up):
         buf, ss, rs = (got_r, r_ss, r_rs) if up else (got_l, l_ss, l_rs)
         to = z + 1 if up else z - 1
         to = jnp.clip(to, 0, n_z - 1)
         return pltpu.make_async_remote_copy(
-            src_ref=term.at[d * fold + y, pl.ds(0, top), :], dst_ref=buf.at[d], send_sem=ss.at[d], recv_sem=rs.at[d],
+            src_ref=term.at[d * fold + y, pl.ds(*halves[h]), :], dst_ref=buf.at[d, pl.ds(*halves[h]), :],
+            send_sem=ss.at[d * 2 + h], recv_sem=rs.at[d * 2 + h],
             device_id=(to * fold + y, t), device_id_type=MESH,
         )
 
-    def add_into(d, buf):
+    def add_into(d, h, buf):
         own = d * fold + y
-        step = max(c for c in range(8, 65, 8) if top % c == 0)
-
-        @pl.loop(0, top // step)
+        first, count = halves[h]
+        step = max(c for c in range(8, 81, 8) if count % c == 0)
+
+        @pl.loop(0, count // step)
         def _(i):
-            at = pl.ds(pl.multiple_of(i * step, 8), step)
+            at = pl.ds(pl.multiple_of(first + i * step, 8), step)
             term[own, at, :] = term[own, at, :] + buf[d, at, :]
 
-    def hop(k):
+    def hop(k, h):
         d = dest[k]
-        y_copies[k].wait_recv()
-        add_into(d, got_y)
+        y_copies[k][h].wait_recv()
+        add_into(d, h, got_y)
 
         @pl.when(d > z)
         def _():
             @pl.when(z > 0)
             def _():
-                line_copy(d, True).wait_recv()
-                add_into(d, got_r)
-
-            line_copy(d, True).start()
+                line_copy(d, h, True).wait_recv()
+                add_into(d, h, got_r)
+
+            line_copy(d, h, True).start()
 
         @pl.when(d < z)
         def _():
             @pl.when(z < n_z - 1)
             def _():
-                line_copy(d, False).wait_recv()
-                add_into(d, got_l)
-
-            line_copy(d, False).start()
+                line_copy(d, h, False).wait_recv()
+                add_into(d, h, got_l)
+
+            line_copy(d, h, False).start()
 
     def low_copy(d, up):
         buf, ss, rs = (low_r, lr_ss, lr_rs) if up else (low_l, ll_ss, ll_rs)
@@ -243,8 +268,8 @@
 
         low_swap.start()
 
-    y_copies[0].start()
-    y_copies[1].start()
+    for h in range(2):
+        y_copies[1][h].start()
 
     @pl.when(jnp.logical_or(z == 0, z == n_z - 1))
     def _():
@@ -307,7 +332,8 @@
         halo.start()
 
     for k in range(2, n_z):
-        y_copies[k].start()
+        for h in range(2):
+            y_copies[k][h].start()
 
     def shift_block(i):
         start = pl.multiple_of(i * reach, reach)
@@ -356,12 +382,16 @@
     def _(i):
         shift_block(i)
 
-    hop(0)
+    marks = [(n_row - 2) * i // 4 for i in range(5)]
+    hop(0, 0)
+    conv_blocks(marks[0], marks[1])
+    hop(0, 1)
     low_end()
-    half = (n_row - 2) // 2
-    conv_blocks(0, half)
-    hop(1)
-    conv_blocks(half, n_row - 2)
+    conv_blocks(marks[1], marks[2])
+    hop(1, 0)
+    conv_blocks(marks[2], marks[3])
+    hop(1, 1)
+    conv_blocks(marks[3], marks[4])
 
     @pl.when(s < n_sp - 1)
     def _():
@@ -391,7 +421,8 @@
     for c in gz_copies:
         c.start()
     for k in range(2, n_z - 1):
-        hop(k)
+        for h in range(2):
+            hop(k, h)
 
     @pl.loop(0, n_blk)
     def _(i):
@@ -412,18 +443,19 @@
         device_id=(z * fold + other_y, t), device_id_type=MESH,
     )
     gy.start()
-    y_copies[n_z - 1].wait_recv()
-    add_into(z, got_y)
-
-    @pl.when(z > 0)
-    def _():
-        line_copy(z, True).wait_recv()
-        add_into(z, got_r)
-
-    @pl.when(z < n_z - 1)
-    def _():
-        line_copy(z, False).wait_recv()
-        add_into(z, got_l)
+    for h in range(2):
+        y_copies[n_z - 1][h].wait_recv()
+        add_into(z, h, got_y)
+
+        @pl.when(z > 0)
+        def _():
+            line_copy(z, h, True).wait_recv()
+            add_into(z, h, got_r)
+
+        @pl.when(z < n_z - 1)
+        def _():
+            line_copy(z, h, False).wait_recv()
+            add_into(z, h, got_l)
 
     low_swap.wait()
     own = z * fold + y
@@ -432,7 +464,8 @@
     gy.wait()
     out_t[...] = ((g_mid[...] + g_yin[...]) * scale)[:n_taps]
     for k in range(n_z):
-        y_copies[k].wait_send()
+        for h in range(2):
+            y_copies[k][h].wait_send()
 
     @pl.when(s > 0)
     def _():
@@ -443,12 +476,14 @@
 
         @pl.when(d > z)
         def _():
-            line_copy(d, True).wait_send()
+            for h in range(2):
+                line_copy(d, h, True).wait_send()
             low_copy(d, True).wait_send()
 
         @pl.when(d < z)
         def _():
-            line_copy(d, False).wait_send()
+            for h in range(2):
+                line_copy(d, h, False).wait_send()
             low_copy(d, False).wait_send()
 
 
@@ -488,7 +523,7 @@
             V((n_taps, 8, ch), f32), V((32, ch), f32), V((32, ch), f32), V((n_z - 1, 32, ch), f32),
             V((32, ch), f32), V((n_taps, 8, ch), f32),
             dma((n_tp - 1,)), dma((n_tp - 1,)), dma((n_tp - 1,)), dma((n_tp - 1,)),
-            dma((n_z,)), dma((n_z,)), dma((n_z,)), dma((n_z,)), dma((n_z,)), dma((n_z,)),
+            *[dma((2 * n_z,))] * 6,
             dma((n_z,)), dma((n_z,)), dma((n_z,)), dma((n_z,)), dma, dma,
             dma, dma, dma((n_z - 1,)), dma((n_z - 1,)), dma, dma,
         ],

time: 64 us -> 61 us (0.953)
  the two profiles are of different devices: /device:TPU:12 before, /device:TPU:8 now
where the time goes in v4:
time: 61 us; the launch traced here: 60.9 us
  Pallas kernels  60.2 us (99%)
  between operations  0.64 us (1%)
    pallas_call x1, Pallas kernels, fused(): pl.pallas_call(functools.partial(kernel, n_sp, n_tp, fold), out_shape=(ja...  58 us
    pallas_call x1, Pallas kernels, fused(): pl.pallas_call(finish, out_shape=tuple((jax.ShapeDtypeStruct(r.shape, r.d...  2.25 us

profile of v4, /device:TPU:8, one launch (start us, length us, event | category | flops | bytes accessed | tf_op | source)
XLA Modules:
  0.0 60.9 jit_solution(13156383820931967950)
XLA Ops:
  0.6 58.0 %shard_map.102 = (bf16[504,512]{1,0:T(8,128)(2,1)}, bf16[504,512]{1,0:T(8,128)(2,1)}, f32[504,252]{1,0:T(8,128)}, f32[31,504]{1,0:T(8,128)}) custom-call(bf16[504,512]{1,0:T(8,128)(2,1)} %bitcast.7, bf16[504,512]{1,0:T(8,128)(2,1)} %bitcast.8, bf16[504,512]{1,0:T(8,128)(2,1)} %bitcast.9, bf16[31,504]{1,0:T(8,128)(2,1)} %taps.1, bf16[504]{0:T(512)(128)(2,1)} %gain.1, ...), custom_call_target="tpu_custom_call" | custom-call | tf_op jit(solution)/shard_map/pallas_call | solution.py:504
  58.6 2.2 %shard_map.103 = (bf16[504,512]{1,0:T(8,128)(2,1)}, bf16[504,512]{1,0:T(8,128)(2,1)}, f32[504,252]{1,0:T(8,128)}, f32[31,504]{1,0:T(8,128)}) custom-call(bf16[504,512]{1,0:T(8,128)(2,1)} %get-tuple-element.12.v_in, bf16[504,512]{1,0:T(8,128)(2,1)} %get-tuple-element.13.g_in, f32[504,252]{1,0:T(8,128)} %get-tuple-element.14.w_in, ...), custom_call_target="tpu_custom_call" | custom-call | tf_op jit(solution)/shard_map/pallas_call | solution.py:538

commit v5 on v4

--- a/solution.py
+++ b/solution.py
@@ -305,6 +305,12 @@
         at = pl.ds(pl.multiple_of(i * blk, blk), blk)
         gated_s[at, :] = (pv[:, at].astype(f32) * jax.nn.sigmoid(pg[:, at].astype(f32))).T
 
+    at_end = jnp.logical_or(z == 0, z == n_z - 1)
+
+    @pl.when(at_end)
+    def _():
+        hop(0, 0)
+
     for c in mom_copies:
         c.wait()
     total = mom[...]
@@ -383,9 +389,21 @@
         shift_block(i)
 
     marks = [(n_row - 2) * i // 4 for i in range(5)]
-    hop(0, 0)
+
+    @pl.when(at_end)
+    def _():
+        hop(0, 1)
+
+    @pl.when(mid)
+    def _():
+        hop(0, 0)
+
     conv_blocks(marks[0], marks[1])
-    hop(0, 1)
+
+    @pl.when(mid)
+    def _():
+        hop(0, 1)
+
     low_end()
     conv_blocks(marks[1], marks[2])
     hop(1, 0)

time: 61 us -> 61 us (level)
  no operation moved by 1% of the time
where the time goes in v5:
time: 61 us; the launch traced here: 60.9 us
  Pallas kernels  60.2 us (99%)
  between operations  0.64 us (1%)
    pallas_call x1, Pallas kernels, fused(): pl.pallas_call(functools.partial(kernel, n_sp, n_tp, fold), out_shape=(ja...  58 us
    pallas_call x1, Pallas kernels, fused(): pl.pallas_call(finish, out_shape=tuple((jax.ShapeDtypeStruct(r.shape, r.d...  2.25 us

profile of v5, /device:TPU:8, one launch (start us, length us, event | category | flops | bytes accessed | tf_op | source)
XLA Modules:
  0.0 60.9 jit_solution(8024965984329993872)
XLA Ops:
  0.6 58.0 %shard_map.102 = (bf16[504,512]{1,0:T(8,128)(2,1)}, bf16[504,512]{1,0:T(8,128)(2,1)}, f32[504,252]{1,0:T(8,128)}, f32[31,504]{1,0:T(8,128)}) custom-call(bf16[504,512]{1,0:T(8,128)(2,1)} %bitcast.7, bf16[504,512]{1,0:T(8,128)(2,1)} %bitcast.8, bf16[504,512]{1,0:T(8,128)(2,1)} %bitcast.9, bf16[31,504]{1,0:T(8,128)(2,1)} %taps.1, bf16[504]{0:T(512)(128)(2,1)} %gain.1, ...), custom_call_target="tpu_custom_call" | custom-call | tf_op jit(solution)/shard_map/pallas_call | solution.py:522
  58.6 2.2 %shard_map.103 = (bf16[504,512]{1,0:T(8,128)(2,1)}, bf16[504,512]{1,0:T(8,128)(2,1)}, f32[504,252]{1,0:T(8,128)}, f32[31,504]{1,0:T(8,128)}) custom-call(bf16[504,512]{1,0:T(8,128)(2,1)} %get-tuple-element.12.v_in, bf16[504,512]{1,0:T(8,128)(2,1)} %get-tuple-element.13.g_in, f32[504,252]{1,0:T(8,128)} %get-tuple-element.14.w_in, ...), custom_call_target="tpu_custom_call" | custom-call | tf_op jit(solution)/shard_map/pallas_call | solution.py:556
